TPU v7x, 128 devices: a whole 4x4x4 slice. The times are simulated.
128 devices in a mesh: ep: 128 (over z, y, x, core).
Axes of the slice: x: 4, y: 4, z: 4, core: 2. Of those that a mesh axis runs over, the one named last changes fastest.
Arguments:
- tokens: bfloat16 [16384, 2048], P('ep'), may hold values from -6 to 6
- norm_gain: float32 [2048], replicated, may hold values from 0.1 to 1.9
- route_ids: int32 [16384, 2], P('ep'), may hold values from 0 to 127, all different within a row; in each aligned block of 128 rows (0 to 127, 128 to 255, ...) at most 8 rows name the same one
- route_weight: float32 [16384, 2], P('ep'), may hold values from 0.25 to 1
- expert_gate: bfloat16 [128, 2048, 1024], P('ep'), may hold values from -0.125 to 0.125
- expert_up: bfloat16 [128, 2048, 1024], P('ep'), may hold values from -0.125 to 0.125
- expert_down: bfloat16 [128, 1024, 2048], P('ep'), may hold values from -0.1875 to 0.1875
- dense_up: bfloat16 [2048, 512], P('ep'), may hold values from -0.125 to 0.125
- dense_down: bfloat16 [512, 2048], P(None, 'ep'), may hold values from -0.25 to 0.25
- branch_gate: float32 [2048], replicated, may hold values from -1.5 to 1.5
Outputs:
- mixed: bfloat16 [16384, 2048], P('ep')
Inputs may be any that keep to these rules, and one draw needn't show every extreme that they name: `route_ids`: each token names 2 different experts; among the 128 tokens of one device (aligned blocks of rows) no expert is named more than 8 times, and in every draw some expert is named exactly 8 times by some device's tokens; every expert is named by some token.
All inputs are finite; a program needn't handle non-finite values.
Results may differ from a plain program's by a relative error of at most 0.01.
Values may be sent and summed in bfloat16 or wider, within the bound.
A program may use at most 128 MiB of HBM per device.

v0:
```python
import functools
import math

import jax
import jax.numpy as jnp
from jax import lax
from jax.experimental import pallas as pl
from jax.experimental.pallas import tpu as pltpu
from jax.sharding import PartitionSpec as P

CAP = 8
F32 = jnp.float32
BF16 = jnp.bfloat16


def xor(a, b, size):
    out, bit = 0, 1
    while bit < size:
        out = out + ((a // bit) % 2 + (b // bit) % 2) % 2 * bit
        bit *= 2
    return out


def kernel(
    dims,
    tokens, gain, ids, weight, w_gate, w_up, w_down, d_up, d_down, branch,
    out,
    normed, send, recv, result, back, v_gate, v_up, v_down, wide,
    local_sem, out_send, out_recv, ret_send, ret_recv,
    w_send, w_recv,
):
    n_z, n_y, n_x, n_c = dims
    plane = n_y * n_x * n_c
    n = n_z * plane
    me = lax.axis_index("ep")
    my_z = me // plane
    my_in = me % plane
    my_c = me % n_c
    my_x = me // n_c % n_x
    my_y = me // (n_c * n_x) % n_y
    rows = tokens.shape[0]
    width = tokens.shape[1]
    experts = n
    slots = experts * CAP

    def dev(z, y, x, c):
        return ((z * n_y + y) * n_x + x) * n_c + c

    barrier = pltpu.get_barrier_semaphore()

    def greet(i, carry):
        pl.semaphore_signal(barrier, inc=1, device_id=((me + i) % n,), device_id_type=pl.DeviceIdType.MESH)
        return carry

    lax.fori_loop(1, n, greet, 0)

    own_up = pltpu.make_async_copy(d_up, wide.at[0, my_z, my_y, my_x, my_c], local_sem.at[0])
    own_down = pltpu.make_async_copy(d_down, wide.at[1, my_z, my_y, my_x, my_c], local_sem.at[1])
    own_up.start()
    own_down.start()
    loads = [
        pltpu.make_async_copy(w_gate.at[0], v_gate, local_sem.at[2]),
        pltpu.make_async_copy(w_up.at[0], v_up, local_sem.at[3]),
        pltpu.make_async_copy(w_down.at[0], v_down, local_sem.at[4]),
    ]
    for load in loads:
        load.start()

    x = tokens[...].astype(F32)
    scale = lax.rsqrt(jnp.mean(x * x, axis=-1, keepdims=True) + 1e-06)
    normed[...] = (x * scale * gain[...]).astype(BF16)

    id0, id1 = ids[0:1, :], ids[1:2, :]
    e_iota = lax.broadcasted_iota(jnp.int32, (experts, rows), 0)
    hot0 = (id0 == e_iota).astype(F32)
    hot1 = (id1 == e_iota).astype(F32)
    before = lax.broadcasted_iota(jnp.int32, (rows, rows), 0) < lax.broadcasted_iota(jnp.int32, (rows, rows), 1)
    count = jnp.dot((hot0 + hot1).astype(BF16), before.astype(F32).astype(BF16), preferred_element_type=F32)
    pos0 = id0 * CAP + jnp.sum(hot0 * count, axis=0, keepdims=True).astype(jnp.int32)
    pos1 = id1 * CAP + jnp.sum(hot1 * count, axis=0, keepdims=True).astype(jnp.int32)
    p_iota = lax.broadcasted_iota(jnp.int32, (slots, rows), 0)
    table0 = (pos0 == p_iota).astype(F32)
    table1 = (pos1 == p_iota).astype(F32)
    place = (table0 + table1).astype(BF16)
    packed = jnp.dot(place, normed[...], preferred_element_type=F32)
    send[...] = packed.reshape(n, CAP, width).astype(BF16)

    own_up.wait()
    own_down.wait()
    pl.semaphore_wait(barrier, n - 1)

    def remote(src, dst, s, r, target):
        return pltpu.make_async_remote_copy(
            src_ref=src, dst_ref=dst, send_sem=s, recv_sem=r,
            device_id=(target,), device_id_type=pl.DeviceIdType.MESH,
        )

    at = (my_z, my_y, my_x, my_c)
    orders = ((0, 1, 2, 3), (0, 2, 1, 3))

    def block_copy(half, stage, d, incoming):
        order = orders[half]
        axis = order[stage]
        origin = (at[axis] + dims[axis] - d) % dims[axis] if incoming else at[axis]
        where = [at[i] for i in range(4)]
        for held in order[:stage]:
            where[held] = slice(None)
        where[axis] = origin
        part = wide.at[(half,) + tuple(where)]
        target = [at[i] for i in range(4)]
        target[axis] = (at[axis] + d) % dims[axis]
        return remote(part, part, w_send.at[half, stage, d], w_recv.at[half, stage, d], dev(*target))

    def each(stage, act, incoming=False):
        for half in range(2):
            for d in range(1, dims[orders[half][stage]]):
                act(block_copy(half, stage, d, incoming))

    def begin(stage):
        each(stage, lambda copy: copy.start())

    def arrive(stage):
        each(stage, lambda copy: copy.wait_recv(), True)

    def leave(stage):
        each(stage, lambda copy: copy.wait_send())

    begin(0)

    def partner(step):
        z = xor(my_z, (step // plane + n_z // 2) % n_z, n_z)
        return z * plane + xor(my_in, step % plane, plane)

    own_step = (n_z - n_z // 2) * plane

    def over_others(first, last, body):
        def guarded(step, carry):
            body(partner(step))
            return carry

        if first <= own_step < last:
            lax.fori_loop(first, own_step, guarded, 0)
            lax.fori_loop(own_step + 1, last, guarded, 0)
        else:
            lax.fori_loop(first, last, guarded, 0)

    def dispatch(target, origin):
        return remote(send.at[target], recv.at[origin], out_send.at[target], out_recv.at[origin], target)

    def giveback(target, origin):
        return remote(result.at[target], back.at[origin], ret_send.at[target], ret_recv.at[origin], target)

    over_others(0, n, lambda t: dispatch(t, me).start())
    recv[me] = send[me]

    for load in loads:
        load.wait()

    def experts_on(phase):
        z = xor(my_z, (phase + n_z // 2) % n_z, n_z)
        block = pl.ds(z * plane, plane)
        x_in = recv[block].reshape(plane * CAP, width)
        gate_part = jnp.dot(x_in, v_gate[...], preferred_element_type=F32)
        up_part = jnp.dot(x_in, v_up[...], preferred_element_type=F32)
        hidden = (gate_part / (1.0 + jnp.exp(-gate_part)) * up_part).astype(BF16)
        res = jnp.dot(hidden, v_down[...], preferred_element_type=F32)
        result[block] = res.reshape(plane, CAP, width).astype(BF16)

    arrive(0)
    begin(1)

    def do_phase(phase):
        lo, hi = phase * plane, (phase + 1) * plane
        over_others(lo, hi, lambda t: dispatch(me, t).wait_recv())
        experts_on(phase)
        over_others(lo, hi, lambda t: giveback(t, me).start())

    for phase in range(n_z):
        do_phase(phase)
        if phase == 0:
            arrive(1)
            begin(2)
        if phase == 2:
            arrive(2)
            begin(3)
        if phase == 3:
            arrive(3)

    back[me] = result[me]

    dense_pre = jnp.dot(normed[...], wide[0].reshape(width, -1), preferred_element_type=F32)
    dense_hidden = (dense_pre / (1.0 + jnp.exp(-dense_pre))).astype(BF16)
    dense_out = lax.dot_general(
        dense_hidden, wide[1].reshape(width, -1), (((1,), (1,)), ((), ())), preferred_element_type=F32
    )
    dense_out = jnp.tanh(branch[...]) * dense_out

    share = table0 * weight[0:1, :] + table1 * weight[1:2, :]
    high = share.astype(BF16)
    low = (share - high.astype(F32)).astype(BF16)

    over_others(0, n, lambda t: giveback(me, t).wait_recv())
    rows_back = back[...].reshape(slots, width)
    across = (((0,), (0,)), ((), ()))
    combined = lax.dot_general(high, rows_back, across, preferred_element_type=F32)
    combined = combined + lax.dot_general(low, rows_back, across, preferred_element_type=F32)
    out[...] = (combined + dense_out).astype(BF16)

    over_others(0, n, lambda t: dispatch(t, me).wait_send())
    over_others(0, n, lambda t: giveback(t, me).wait_send())
    for stage in range(4):
        leave(stage)


def on_device(tokens, norm_gain, route_ids, route_weight, expert_gate, expert_up, expert_down, dense_up, dense_down, branch_gate):
    n = lax.axis_size("ep")
    assert expert_gate.shape[0] == 1
    rows, width = tokens.shape
    ff = expert_gate.shape[2]
    d_rows, dh = dense_up.shape
    n_z = 4
    side = math.isqrt(n // n_z // 2)
    dims = (n_z, side, side, 2)
    assert math.prod(dims) == n
    vmem = pl.BlockSpec(memory_space=pltpu.VMEM)
    hbm = pl.BlockSpec(memory_space=pl.ANY)
    dma = pltpu.SemaphoreType.DMA
    return pl.pallas_call(
        functools.partial(kernel, dims),
        out_shape=jax.ShapeDtypeStruct((rows, width), BF16),
        in_specs=[vmem, vmem, vmem, vmem, hbm, hbm, hbm, hbm, hbm, vmem],
        out_specs=vmem,
        scratch_shapes=[
            pltpu.VMEM((rows, width), BF16),
            pltpu.VMEM((n, CAP, width), BF16),
            pltpu.VMEM((n, CAP, width), BF16),
            pltpu.VMEM((n, CAP, width), BF16),
            pltpu.VMEM((n, CAP, width), BF16),
            pltpu.VMEM((width, ff), BF16),
            pltpu.VMEM((width, ff), BF16),
            pltpu.VMEM((ff, width), BF16),
            pltpu.VMEM((2,) + dims + (d_rows, dh), BF16),
            dma((5,)), dma((n,)), dma((n,)), dma((n,)), dma((n,)),
            dma((2, 4, n_z)), dma((2, 4, n_z)),
        ],
        compiler_params=pltpu.CompilerParams(
            collective_id=0, has_side_effects=True, vmem_limit_bytes=60 * 1024 * 1024
        ),
    )(
        tokens, norm_gain.reshape(1, -1), route_ids.T, route_weight.T,
        expert_gate, expert_up, expert_down, dense_up, dense_down.T, branch_gate.reshape(1, -1),
    )


def solution(mesh):
    placed = (
        P("ep", None), P(), P("ep", None), P("ep", None),
        P("ep", None, None), P("ep", None, None), P("ep", None, None),
        P("ep", None), P(None, "ep"), P(),
    )
    return jax.shard_map(
        on_device, mesh=mesh, in_specs=placed, out_specs=P("ep", None), check_vma=False
    )
```

profile of v0, /device:TPU:43, one launch (start us, length us, event | category | flops | bytes accessed | tf_op | source)
XLA Modules:
  0.0 169.5 jit_solution(5757276066123286832)
XLA Ops:
  0.0 167.6 %shard_map.100 = bf16[128,2048]{1,0:T(8,128)(2,1)} custom-call(bf16[128,2048]{1,0:T(8,128)(2,1)} %tokens.1, f32[1,2048]{1,0:T(1,128)} %bitcast.6, s32[2,128]{1,0:T(2,128)} %bitcast.8, f32[2,128]{1,0:T(2,128)} %bitcast.9, bf16[1,2048,1024]{2,1,0:T(8,128)(2,1)} %w_gate.1, bf16[1,2048,1024]{2,1,0:T(8,128)(2,1)} %w_up.1, bf16[1,1024,2048]{2,1,0:T(8,128)(2,1)} %w_down.1, ...), custom_call_target="tpu_custom_call" | custom-call | tf_op jit(solution)/shard_map/pallas_call | solution.py:228
  167.6 1.9 %copy.12 = bf16[128,2048]{1,0:T(8,128)(2,1)} copy(bf16[128,2048]{1,0:T(8,128)(2,1)} %shard_map.100) | data formatting | bytes 1048576
where the time goes:
time: 170 us; the launch traced here: 169 us
  Pallas kernels  168 us (99%)
  local copies, waits for them, and re-layouts  1.88 us (1%)
    pallas_call x1, Pallas kernels, on_device(): pl.pallas_call(functools.partial(kernel, dims), out_shape=jax.ShapeDtypeS...  168 us

commit v1 on v0

v1 whole, which is shorter than its diff:
```python
import functools
import itertools
import math

import jax
import jax.numpy as jnp
from jax import lax
from jax.experimental import pallas as pl
from jax.experimental.pallas import tpu as pltpu
from jax.sharding import PartitionSpec as P

CAP = 8
F32 = jnp.float32
BF16 = jnp.bfloat16


def plane_order(side, cores):
    def hop(d):
        return min(d, side - d)

    offsets = [o for o in itertools.product(range(side), range(side), range(cores)) if any(o)]
    order = []
    for o in sorted(offsets, key=lambda o: hop(o[0]) + hop(o[1])):
        for pick in (o, (-o[0] % side, -o[1] % side, o[2])):
            if pick not in order:
                order.append(pick)
    return order


def with_dim(k, d, a, b, e):
    full = [a, b]
    full.insert(k, d)
    return (*full, e)


def kernel(
    side, cores, cols,
    tokens, gain, ids, weight, w_gate, w_up, w_down, d_up, d_down, branch,
    out,
    ag, mine, info, send, recv, result, back, rs_out, rs_in, high_t, low_t, v_gate, v_up, v_down, wide,
    local_sem, info_send, info_recv, ag_send, ag_recv, out_send, out_recv, own_sem,
    ret_send, ret_recv, rs_send, rs_recv, w_send, w_recv,
):
    rows, width = tokens.shape
    plane = side * side * cores
    n = side * plane
    slots = plane * CAP
    me = lax.axis_index("ep")
    dims = (side, side, side, cores)
    strides = (plane, side * cores, cores, 1)
    at = tuple(me // strides[i] % dims[i] for i in range(4))
    part = [[(at[i] + d) % dims[i] * strides[i] for d in range(dims[i])] for i in range(4)]
    grid = (side, side, side, cores, CAP, width)
    send6, recv6, result6, back6 = (r.reshape(*grid) for r in (send, recv, result, back))
    ring = sorted(range(1, side), key=lambda d: (min(d, side - d), d))
    others = pl.ds(1, side - 1)
    order = plane_order(side, cores)
    peers = len(order)
    lanes = [pl.ds(lo, hi - lo) for lo, hi in cols]

    def dev(o):
        return part[0][o[0]] + part[1][o[1]] + part[2][o[2]] + part[3][o[3]]

    def minus(o):
        return tuple(-o[i] % dims[i] for i in range(4))

    def along(k, d):
        return tuple(d if i == k else 0 for i in range(4))

    def remote(src, dst, s, r, target):
        return pltpu.make_async_remote_copy(
            src_ref=src, dst_ref=dst, send_sem=s, recv_sem=r,
            device_id=(target,), device_id_type=pl.DeviceIdType.MESH,
        )

    near = dev((0, 0, 0, 1))

    barrier = pltpu.get_barrier_semaphore()
    greeted = sorted({with_dim(k, 0, *o) for k in range(3) for o in order})
    for o in greeted:
        pl.semaphore_signal(barrier, inc=1, device_id=(dev(o),), device_id_type=pl.DeviceIdType.MESH)

    own_up = pltpu.make_async_copy(d_up, wide.at[(0, *at)], local_sem.at[0])
    own_down = pltpu.make_async_copy(d_down, wide.at[(1, *at)], local_sem.at[1])
    own_up.start()
    own_down.start()
    loads = [
        pltpu.make_async_copy(w_gate.at[0], v_gate, local_sem.at[2]),
        pltpu.make_async_copy(w_up.at[0], v_up, local_sem.at[3]),
        pltpu.make_async_copy(w_down.at[0], v_down, local_sem.at[4]),
    ]
    for load in loads:
        load.start()

    x = tokens[...].astype(F32)
    scale = lax.rsqrt(jnp.mean(x * x, axis=-1, keepdims=True) + 1e-06)
    ag[0] = (x * scale * gain[...]).astype(BF16)
    mine[...] = jnp.concatenate(
        [ids[...].astype(F32), weight[...], jnp.zeros((4, rows), F32)], axis=0
    )

    before = lax.broadcasted_iota(jnp.int32, (rows, rows), 0) < lax.broadcasted_iota(jnp.int32, (rows, rows), 1)
    before = before.astype(F32).astype(BF16)
    j_iota = lax.broadcasted_iota(jnp.int32, (plane, rows), 0)
    p_iota = lax.broadcasted_iota(jnp.int32, (slots, rows), 0)

    def slots_of(k, facts):
        first, second = [i for i in range(3) if i != k]

        def local(expert):
            coords = [expert // strides[i] % dims[i] for i in range(4)]
            away = [(coords[i] + dims[i] - at[i]) % dims[i] for i in range(4)]
            j = (away[first] * side + away[second]) * cores + away[3]
            return jnp.where(away[k] == 0, j, -1)

        j0 = local(facts[0:1, :].astype(jnp.int32))
        j1 = local(facts[1:2, :].astype(jnp.int32))
        hot0 = (j0 == j_iota).astype(F32)
        hot1 = (j1 == j_iota).astype(F32)
        count = jnp.dot((hot0 + hot1).astype(BF16), before, preferred_element_type=F32)
        rank0 = jnp.sum(hot0 * count, axis=0, keepdims=True).astype(jnp.int32)
        rank1 = jnp.sum(hot1 * count, axis=0, keepdims=True).astype(jnp.int32)
        slot0 = jnp.where(j0 < 0, -1, j0 * CAP + rank0)
        slot1 = jnp.where(j1 < 0, -1, j1 * CAP + rank1)
        return slot0 == p_iota, slot1 == p_iota

    def pack(k, d, facts):
        lo, hi = cols[k]
        table0, table1 = slots_of(k, facts)
        place = jnp.where(table0 | table1, 1.0, 0.0).astype(BF16)
        packed = jnp.dot(place, ag[d, :, lo:hi], preferred_element_type=F32)
        send[d * plane:(d + 1) * plane, :, lo:hi] = packed.reshape(plane, CAP, hi - lo).astype(BF16)
        share = jnp.where(table0, facts[2:3, :], 0.0) + jnp.where(table1, facts[3:4, :], 0.0)
        share = share.T
        high = share.astype(BF16)
        high_t[k, d] = high
        low_t[k, d] = (share - high.astype(F32)).astype(BF16)

    def sources(k, group, j):
        return with_dim(k, 0 if group == 0 else others, *j)

    def slot_rows(group, j):
        return (0 if group == 0 else others, *j)

    def dispatch(k, group, j):
        return remote(
            send6.at[(*slot_rows(group, j), slice(None), lanes[k])],
            recv6.at[(*sources(k, group, j), slice(None), lanes[k])],
            out_send.at[group, k], out_recv.at[group, k], dev(with_dim(k, 0, *j)),
        )

    here = (0, 0, 0)

    def keep(k, group):
        return pltpu.make_async_copy(
            send6.at[(*slot_rows(group, here), slice(None), lanes[k])],
            recv6.at[(*sources(k, group, here), slice(None), lanes[k])],
            own_sem.at[group, k],
        )

    def start_group(group):
        for i in range(peers):
            for k in range(3):
                dispatch(k, group, order[(i + k * 10) % peers]).start()
        for k in range(3):
            keep(k, group).start()

    def bulk(buffer, k, blocks, s, r):
        part_of = buffer.at[pl.ds(0, blocks), :, lanes[k]]
        return remote(part_of, part_of, s, r, near)

    for k in range(3):
        pack(k, 0, mine)

    own_up.wait()
    own_down.wait()
    pl.semaphore_wait(barrier, len(greeted))

    def tell(k, d):
        return remote(mine, info.at[k, d], info_send.at[k, d], info_recv.at[k, d], dev(along(k, d)))

    def share_tokens(k, d):
        return remote(
            ag.at[0, :, lanes[k]], ag.at[d, :, lanes[k]], ag_send.at[k, d], ag_recv.at[k, d], dev(along(k, d))
        )

    for d in ring:
        for k in range(3):
            tell(k, d).start()
    for d in ring:
        for k in range(3):
            share_tokens(k, d).start()

    pieces = (
        (0, 0, 384, (0, 1, 2, 3)),
        (0, 384, 512, (1, 2, 0, 3)),
        (1, 0, 256, (1, 2, 0, 3)),
        (1, 256, 512, (2, 0, 1, 3)),
    )

    def piece_copy(p, stage, d, incoming):
        half, lo, hi, turn = pieces[p]
        axis = turn[stage]
        where = list(at)
        for held in turn[:stage]:
            where[held] = slice(None)
        if incoming:
            where[axis] = (at[axis] + dims[axis] - d) % dims[axis]
        block = wide.at[(half, *where, slice(None), pl.ds(lo, hi - lo))]
        offset = along(axis, d)
        return remote(block, block, w_send.at[p, stage, d], w_recv.at[p, stage, d], dev(offset))

    def each(stage, act, incoming=False):
        for p in range(4):
            axis = pieces[p][3][stage]
            for d in range(1, dims[axis]):
                act(piece_copy(p, stage, d, incoming))

    def begin(stage):
        each(stage, lambda copy: copy.start())

    def arrive(stage):
        each(stage, lambda copy: copy.wait_recv(), True)

    def leave(stage):
        each(stage, lambda copy: copy.wait_send())

    begin(0)
    start_group(0)

    for d in ring:
        for k in range(3):
            tell(k, d).wait_recv()
            share_tokens(k, d).wait_recv()
            pack(k, d, info[k, d])
    start_group(1)

    arrive(0)
    begin(1)

    for load in loads:
        load.wait()

    def experts_on(p):
        block = pl.ds(p * plane, plane)
        x_in = recv[block].reshape(plane * CAP, width)
        gate_part = jnp.dot(x_in, v_gate[...], preferred_element_type=F32)
        up_part = jnp.dot(x_in, v_up[...], preferred_element_type=F32)
        hidden = (gate_part / (1.0 + jnp.exp(-gate_part)) * up_part).astype(BF16)
        res = jnp.dot(hidden, v_down[...], preferred_element_type=F32)
        result[block] = res.reshape(plane, CAP, width).astype(BF16)

    for group in range(2):
        for k in range(3):
            keep(k, group).wait()
            blocks = peers * (1 if group == 0 else side - 1)
            bulk(recv, k, blocks, out_send.at[group, k], out_recv.at[group, k]).wait_recv()

    arrive(1)
    begin(2)

    def giveback(k, d, j):
        group = 0 if isinstance(d, int) and d == 0 else 1
        there = minus(with_dim(k, 0, *j))
        src = result6.at[(*with_dim(k, d, *j), slice(None), lanes[k])]
        dst = back6.at[(d, *j, slice(None), lanes[k])]
        if j == here:
            return pltpu.make_async_copy(src, dst, own_sem.at[2, k] if group == 0 else own_sem.at[3, k])
        return remote(src, dst, ret_send.at[group, k], ret_recv.at[group, k], dev(there))

    spread = [here, *order]
    for p in (*ring, 0):
        experts_on(p)
        flat = [j for j in spread if j[0] == p]
        moves = [(1, others, j) for j in flat] + [(2, others, j) for j in flat]
        moves = [m for pair in zip(moves[:len(flat)], moves[len(flat):]) for m in pair]
        if p:
            moves += [(0, p, j) for j in spread if j != here]
        for k, d, j in moves:
            giveback(k, d, j).start()
    for j in order:
        for k in range(3):
            giveback(k, 0, j).start()
    for k in range(3):
        giveback(k, 0, here).start()
    keep_back = pltpu.make_async_copy(
        result6.at[(*with_dim(0, others, *here), slice(None), lanes[0])],
        back6.at[(others, *here, slice(None), lanes[0])], own_sem.at[3, 0],
    )
    keep_back.start()

    arrive(2)
    begin(3)

    def combine(k, d):
        lo, hi = cols[k]
        rows_back = back[d * plane:(d + 1) * plane, :, lo:hi].reshape(slots, hi - lo)
        total = jnp.dot(high_t[k, d], rows_back, preferred_element_type=F32)
        return total + jnp.dot(low_t[k, d], rows_back, preferred_element_type=F32)

    def partial(k, d):
        return remote(
            rs_out.at[d, :, lanes[k]], rs_in.at[d, :, lanes[k]], rs_send.at[k, d], rs_recv.at[k, d],
            dev(along(k, -d % side)),
        )

    keep_back.wait()
    for k in range(3):
        if k:
            giveback(k, others, here).wait()
        bulk(back, k, peers * (side - 1), ret_send.at[1, k], ret_recv.at[1, k]).wait_recv()
        for d in ring:
            lo, hi = cols[k]
            rs_out[d, :, lo:hi] = combine(k, d).astype(BF16)
            partial(k, d).start()

    arrive(3)
    dense_pre = jnp.dot(ag[0], wide[0].reshape(width, -1), preferred_element_type=F32)
    dense_hidden = (dense_pre / (1.0 + jnp.exp(-dense_pre))).astype(BF16)

    for k in range(3):
        lo, hi = cols[k]
        giveback(k, 0, here).wait()
        bulk(back, k, peers, ret_send.at[0, k], ret_recv.at[0, k]).wait_recv()
    dense_out = lax.dot_general(
        dense_hidden, wide[1].reshape(width, -1), (((1,), (1,)), ((), ())), preferred_element_type=F32
    )
    dense_out = jnp.tanh(branch[...]) * dense_out
    for k in range(3):
        lo, hi = cols[k]
        total = combine(k, 0) + dense_out[:, lo:hi]
        for d in ring:
            partial(k, d).wait_recv()
            total = total + rs_in[d, :, lo:hi].astype(F32)
        out[:, lo:hi] = total.astype(BF16)

    for k in range(3):
        for d in ring:
            tell(k, d).wait_send()
            share_tokens(k, d).wait_send()
            partial(k, d).wait_send()
        for group in range(2):
            blocks = peers * (1 if group == 0 else side - 1)
            bulk(send, k, blocks, out_send.at[group, k], out_recv.at[group, k]).wait_send()
            bulk(result, k, blocks, ret_send.at[group, k], ret_recv.at[group, k]).wait_send()
    for stage in range(4):
        leave(stage)


def on_device(tokens, norm_gain, route_ids, route_weight, expert_gate, expert_up, expert_down, dense_up, dense_down, branch_gate):
    n = lax.axis_size("ep")
    assert expert_gate.shape[0] == 1
    rows, width = tokens.shape
    ff = expert_gate.shape[2]
    d_rows, dh = dense_up.shape
    cores = 2
    side = round((n // cores) ** (1 / 3))
    assert side ** 3 * cores == n
    tile = width // 128
    cuts = [tile // 3, tile // 3 * 2, tile]
    cols = tuple((lo * 128, hi * 128) for lo, hi in zip([0, *cuts[:2]], cuts))
    plane = n // side
    vmem = pl.BlockSpec(memory_space=pltpu.VMEM)
    hbm = pl.BlockSpec(memory_space=pl.ANY)
    dma = pltpu.SemaphoreType.DMA
    return pl.pallas_call(
        functools.partial(kernel, side, cores, cols),
        out_shape=jax.ShapeDtypeStruct((rows, width), BF16),
        in_specs=[vmem, vmem, vmem, vmem, hbm, hbm, hbm, hbm, hbm, vmem],
        out_specs=vmem,
        scratch_shapes=[
            pltpu.VMEM((side, rows, width), BF16),
            pltpu.VMEM((8, rows), F32),
            pltpu.VMEM((3, side, 8, rows), F32),
            pltpu.VMEM((n, CAP, width), BF16),
            pltpu.VMEM((n, CAP, width), BF16),
            pltpu.VMEM((n, CAP, width), BF16),
            pltpu.VMEM((n, CAP, width), BF16),
            pltpu.VMEM((side, rows, width), BF16),
            pltpu.VMEM((side, rows, width), BF16),
            pltpu.VMEM((3, side, rows, plane * CAP), BF16),
            pltpu.VMEM((3, side, rows, plane * CAP), BF16),
            pltpu.VMEM((width, ff), BF16),
            pltpu.VMEM((width, ff), BF16),
            pltpu.VMEM((ff, width), BF16),
            pltpu.VMEM((2, side, side, side, cores, d_rows, dh), BF16),
            dma((5,)), dma((3, side)), dma((3, side)), dma((3, side)), dma((3, side)),
            dma((2, 3)), dma((2, 3)), dma((4, 3)),
            dma((2, 3)), dma((2, 3)), dma((3, side)), dma((3, side)),
            dma((4, 4, side)), dma((4, 4, side)),
        ],
        compiler_params=pltpu.CompilerParams(
            collective_id=0, has_side_effects=True, vmem_limit_bytes=62 * 1024 * 1024
        ),
    )(
        tokens, norm_gain.reshape(1, -1), route_ids.T, route_weight.T,
        expert_gate, expert_up, expert_down, dense_up, dense_down.T, branch_gate.reshape(1, -1),
    )


def solution(mesh):
    placed = (
        P("ep", None), P(), P("ep", None), P("ep", None),
        P("ep", None, None), P("ep", None, None), P("ep", None, None),
        P("ep", None), P(None, "ep"), P(),
    )
    return jax.shard_map(
        on_device, mesh=mesh, in_specs=placed, out_specs=P("ep", None), check_vma=False
    )
```

time: 170 us -> 116 us (0.68)
  the two profiles are of different devices: /device:TPU:43 before, /device:TPU:1 now
where the time goes in v1:
time: 116 us; the launch traced here: 115 us
  Pallas kernels  113 us (97%)
  local copies, waits for them, and re-layouts  1.88 us (2%)
    pallas_call x1, Pallas kernels, on_device(): pl.pallas_call(functools.partial(kernel, side, cores, cols), out_shape=ja...  113 us

profile of v1, /device:TPU:1, one launch (start us, length us, event | category | flops | bytes accessed | tf_op | source)
XLA Modules:
  0.0 114.7 jit_solution(16412455920902799817)
XLA Ops:
  0.0 112.8 %shard_map.100 = bf16[128,2048]{1,0:T(8,128)(2,1)} custom-call(bf16[128,2048]{1,0:T(8,128)(2,1)} %tokens.1, f32[1,2048]{1,0:T(1,128)} %bitcast.6, s32[2,128]{1,0:T(2,128)} %bitcast.8, f32[2,128]{1,0:T(2,128)} %bitcast.9, bf16[1,2048,1024]{2,1,0:T(8,128)(2,1)} %w_gate.1, bf16[1,2048,1024]{2,1,0:T(8,128)(2,1)} %w_up.1, bf16[1,1024,2048]{2,1,0:T(8,128)(2,1)} %w_down.1, ...), custom_call_target="tpu_custom_call" | custom-call | tf_op jit(solution)/shard_map/pallas_call | solution.py:366
  112.8 1.9 %copy.12 = bf16[128,2048]{1,0:T(8,128)(2,1)} copy(bf16[128,2048]{1,0:T(8,128)(2,1)} %shard_map.100) | data formatting | bytes 1048576

commit v2 on v1

--- a/solution.py
+++ b/solution.py
@@ -37,8 +37,8 @@
     side, cores, cols,
     tokens, gain, ids, weight, w_gate, w_up, w_down, d_up, d_down, branch,
     out,
-    ag, mine, info, send, recv, result, back, rs_out, rs_in, high_t, low_t, v_gate, v_up, v_down, wide,
-    local_sem, info_send, info_recv, ag_send, ag_recv, out_send, out_recv, own_sem,
+    ag, mine, info, send, recv, result, back, rs_out, rs_in, high_t, low_t, dense, v_gate, v_up, v_down, wide,
+    ready, local_sem, info_send, info_recv, ag_send, ag_recv, out_send, out_recv, own_sem,
     ret_send, ret_recv, rs_send, rs_recv, w_send, w_recv,
 ):
     rows, width = tokens.shape
@@ -51,11 +51,14 @@
     at = tuple(me // strides[i] % dims[i] for i in range(4))
     part = [[(at[i] + d) % dims[i] * strides[i] for d in range(dims[i])] for i in range(4)]
     grid = (side, side, side, cores, CAP, width)
-    send6, recv6, result6, back6 = (r.reshape(*grid) for r in (send, recv, result, back))
+    by_core = (cores, side, side, side, CAP, width)
+    send6, back6 = (r.reshape(*grid) for r in (send, back))
+    recv6, result6 = (r.reshape(*by_core) for r in (recv, result))
     ring = sorted(range(1, side), key=lambda d: (min(d, side - d), d))
     others = pl.ds(1, side - 1)
     order = plane_order(side, cores)
     peers = len(order)
+    of_core = [[o for o in order if o[2] == e] for e in range(cores)]
     lanes = [pl.ds(lo, hi - lo) for lo, hi in cols]
 
     def dev(o):
@@ -76,9 +79,14 @@
     near = dev((0, 0, 0, 1))
 
     barrier = pltpu.get_barrier_semaphore()
-    greeted = sorted({with_dim(k, 0, *o) for k in range(3) for o in order})
-    for o in greeted:
-        pl.semaphore_signal(barrier, inc=1, device_id=(dev(o),), device_id_type=pl.DeviceIdType.MESH)
+    line = [along(k, d) for d in ring for k in range(3)]
+    greeted = line + [(*o[:3], 1) for o in line] + [(0, 0, 0, 1)]
+
+    def greet(semaphore, offsets):
+        for o in offsets:
+            pl.semaphore_signal(semaphore, inc=1, device_id=(dev(o),), device_id_type=pl.DeviceIdType.MESH)
+
+    greet(barrier, greeted)
 
     own_up = pltpu.make_async_copy(d_up, wide.at[(0, *at)], local_sem.at[0])
     own_down = pltpu.make_async_copy(d_down, wide.at[(1, *at)], local_sem.at[1])
@@ -136,8 +144,11 @@
         high_t[k, d] = high
         low_t[k, d] = (share - high.astype(F32)).astype(BF16)
 
+    def core_first(o):
+        return (o[3], *o[:3])
+
     def sources(k, group, j):
-        return with_dim(k, 0 if group == 0 else others, *j)
+        return core_first(with_dim(k, 0 if group == 0 else others, *j))
 
     def slot_rows(group, j):
         return (0 if group == 0 else others, *j)
@@ -146,7 +157,8 @@
         return remote(
             send6.at[(*slot_rows(group, j), slice(None), lanes[k])],
             recv6.at[(*sources(k, group, j), slice(None), lanes[k])],
-            out_send.at[group, k], out_recv.at[group, k], dev(with_dim(k, 0, *j)),
+            out_send.at[group + j[2] * (group > 0), k], out_recv.at[group + j[2] * (group > 0), k],
+            dev(with_dim(k, 0, *j)),
         )
 
     here = (0, 0, 0)
@@ -158,12 +170,11 @@
             own_sem.at[group, k],
         )
 
-    def start_group(group):
-        for i in range(peers):
+    def start_group(group, targets):
+        count = len(targets)
+        for i in range(count):
             for k in range(3):
-                dispatch(k, group, order[(i + k * 10) % peers]).start()
-        for k in range(3):
-            keep(k, group).start()
+                dispatch(k, group, targets[(i + k * count // 3) % count]).start()
 
     def bulk(buffer, k, blocks, s, r):
         part_of = buffer.at[pl.ds(0, blocks), :, lanes[k]]
@@ -175,6 +186,7 @@
     own_up.wait()
     own_down.wait()
     pl.semaphore_wait(barrier, len(greeted))
+    greet(ready, line)
 
     def tell(k, d):
         return remote(mine, info.at[k, d], info_send.at[k, d], info_recv.at[k, d], dev(along(k, d)))
@@ -226,68 +238,72 @@
         each(stage, lambda copy: copy.wait_send())
 
     begin(0)
-    start_group(0)
+    pl.semaphore_wait(ready, len(line))
+    start_group(0, order)
+    for k in range(3):
+        keep(k, 0).start()
 
     for d in ring:
         for k in range(3):
             tell(k, d).wait_recv()
             share_tokens(k, d).wait_recv()
             pack(k, d, info[k, d])
-    start_group(1)
-
-    arrive(0)
-    begin(1)
+        if d == ring[0]:
+            arrive(0)
+            begin(1)
+    for e in range(cores):
+        start_group(1, of_core[e])
+    for k in range(3):
+        keep(k, 1).start()
+    arrive(1)
+    begin(2)
 
     for load in loads:
         load.wait()
 
+    part_rows = n // (2 * cores)
+
     def experts_on(p):
-        block = pl.ds(p * plane, plane)
-        x_in = recv[block].reshape(plane * CAP, width)
+        block = pl.ds(p * part_rows, part_rows)
+        x_in = recv[block].reshape(part_rows * CAP, width)
         gate_part = jnp.dot(x_in, v_gate[...], preferred_element_type=F32)
         up_part = jnp.dot(x_in, v_up[...], preferred_element_type=F32)
         hidden = (gate_part / (1.0 + jnp.exp(-gate_part)) * up_part).astype(BF16)
         res = jnp.dot(hidden, v_down[...], preferred_element_type=F32)
-        result[block] = res.reshape(plane, CAP, width).astype(BF16)
-
-    for group in range(2):
-        for k in range(3):
-            keep(k, group).wait()
-            blocks = peers * (1 if group == 0 else side - 1)
-            bulk(recv, k, blocks, out_send.at[group, k], out_recv.at[group, k]).wait_recv()
-
-    arrive(1)
-    begin(2)
+        result[block] = res.reshape(part_rows, CAP, width).astype(BF16)
 
     def giveback(k, d, j):
         group = 0 if isinstance(d, int) and d == 0 else 1
         there = minus(with_dim(k, 0, *j))
-        src = result6.at[(*with_dim(k, d, *j), slice(None), lanes[k])]
+        src = result6.at[(*core_first(with_dim(k, d, *j)), slice(None), lanes[k])]
         dst = back6.at[(d, *j, slice(None), lanes[k])]
         if j == here:
             return pltpu.make_async_copy(src, dst, own_sem.at[2, k] if group == 0 else own_sem.at[3, k])
         return remote(src, dst, ret_send.at[group, k], ret_recv.at[group, k], dev(there))
 
-    spread = [here, *order]
-    for p in (*ring, 0):
-        experts_on(p)
-        flat = [j for j in spread if j[0] == p]
-        moves = [(1, others, j) for j in flat] + [(2, others, j) for j in flat]
-        moves = [m for pair in zip(moves[:len(flat)], moves[len(flat):]) for m in pair]
-        if p:
-            moves += [(0, p, j) for j in spread if j != here]
-        for k, d, j in moves:
-            giveback(k, d, j).start()
-    for j in order:
+    def wait_group(group, k, blocks):
+        bulk(recv, k, blocks, out_send.at[group, k], out_recv.at[group, k]).wait_recv()
+
+    def start_back(d, targets):
+        count = len(targets)
+        for i in range(count):
+            for k in range(3):
+                giveback(k, d, targets[(i + k * count // 3) % count]).start()
+
+    for e in range(cores):
         for k in range(3):
-            giveback(k, 0, j).start()
-    for k in range(3):
+            if e == 0:
+                keep(k, 0).wait()
+                keep(k, 1).wait()
+                wait_group(0, k, peers)
+            wait_group(1 + e, k, len(of_core[e]) * (side - 1))
+        for p in range(2):
+            experts_on(e * 2 + p)
+        start_back(others, of_core[e])
+    start_back(0, order)
+    for k in range(3):
+        giveback(k, others, here).start()
         giveback(k, 0, here).start()
-    keep_back = pltpu.make_async_copy(
-        result6.at[(*with_dim(0, others, *here), slice(None), lanes[0])],
-        back6.at[(others, *here, slice(None), lanes[0])], own_sem.at[3, 0],
-    )
-    keep_back.start()
 
     arrive(2)
     begin(3)
@@ -304,10 +320,8 @@
             dev(along(k, -d % side)),
         )
 
-    keep_back.wait()
-    for k in range(3):
-        if k:
-            giveback(k, others, here).wait()
+    for k in range(3):
+        giveback(k, others, here).wait()
         bulk(back, k, peers * (side - 1), ret_send.at[1, k], ret_recv.at[1, k]).wait_recv()
         for d in ring:
             lo, hi = cols[k]
@@ -317,18 +331,15 @@
     arrive(3)
     dense_pre = jnp.dot(ag[0], wide[0].reshape(width, -1), preferred_element_type=F32)
     dense_hidden = (dense_pre / (1.0 + jnp.exp(-dense_pre))).astype(BF16)
-
+    dense_out = lax.dot_general(
+        dense_hidden, wide[1].reshape(width, -1), (((1,), (1,)), ((), ())), preferred_element_type=F32
+    )
+    dense[...] = jnp.tanh(branch[...]) * dense_out
     for k in range(3):
         lo, hi = cols[k]
         giveback(k, 0, here).wait()
         bulk(back, k, peers, ret_send.at[0, k], ret_recv.at[0, k]).wait_recv()
-    dense_out = lax.dot_general(
-        dense_hidden, wide[1].reshape(width, -1), (((1,), (1,)), ((), ())), preferred_element_type=F32
-    )
-    dense_out = jnp.tanh(branch[...]) * dense_out
-    for k in range(3):
-        lo, hi = cols[k]
-        total = combine(k, 0) + dense_out[:, lo:hi]
+        total = combine(k, 0) + dense[:, lo:hi]
         for d in ring:
             partial(k, d).wait_recv()
             total = total + rs_in[d, :, lo:hi].astype(F32)
@@ -339,9 +350,12 @@
             tell(k, d).wait_send()
             share_tokens(k, d).wait_send()
             partial(k, d).wait_send()
+        for e in range(cores):
+            blocks = len(of_core[e]) * (side - 1)
+            bulk(send, k, blocks, out_send.at[1 + e, k], out_recv.at[1 + e, k]).wait_send()
+        bulk(send, k, peers, out_send.at[0, k], out_recv.at[0, k]).wait_send()
         for group in range(2):
             blocks = peers * (1 if group == 0 else side - 1)
-            bulk(send, k, blocks, out_send.at[group, k], out_recv.at[group, k]).wait_send()
             bulk(result, k, blocks, ret_send.at[group, k], ret_recv.at[group, k]).wait_send()
     for stage in range(4):
         leave(stage)
@@ -380,12 +394,14 @@
             pltpu.VMEM((side, rows, width), BF16),
             pltpu.VMEM((3, side, rows, plane * CAP), BF16),
             pltpu.VMEM((3, side, rows, plane * CAP), BF16),
+            pltpu.VMEM((rows, width), F32),
             pltpu.VMEM((width, ff), BF16),
             pltpu.VMEM((width, ff), BF16),
             pltpu.VMEM((ff, width), BF16),
             pltpu.VMEM((2, side, side, side, cores, d_rows, dh), BF16),
+            pltpu.SemaphoreType.REGULAR,
             dma((5,)), dma((3, side)), dma((3, side)), dma((3, side)), dma((3, side)),
-            dma((2, 3)), dma((2, 3)), dma((4, 3)),
+            dma((1 + cores, 3)), dma((1 + cores, 3)), dma((4, 3)),
             dma((2, 3)), dma((2, 3)), dma((3, side)), dma((3, side)),
             dma((4, 4, side)), dma((4, 4, side)),
         ],

time: 116 us -> 107 us (0.922)
  the two profiles are of different devices: /device:TPU:1 before, /device:TPU:8 now
where the time goes in v2:
time: 107 us; the launch traced here: 106 us
  Pallas kernels  105 us (98%)
  local copies, waits for them, and re-layouts  1.88 us (2%)
    pallas_call x1, Pallas kernels, on_device(): pl.pallas_call(functools.partial(kernel, side, cores, cols), out_shape=ja...  105 us

profile of v2, /device:TPU:8, one launch (start us, length us, event | category | flops | bytes accessed | tf_op | source)
XLA Modules:
  0.0 106.5 jit_solution(1551129642535238566)
XLA Ops:
  0.0 104.6 %shard_map.100 = bf16[128,2048]{1,0:T(8,128)(2,1)} custom-call(bf16[128,2048]{1,0:T(8,128)(2,1)} %tokens.1, f32[1,2048]{1,0:T(1,128)} %bitcast.6, s32[2,128]{1,0:T(2,128)} %bitcast.8, f32[2,128]{1,0:T(2,128)} %bitcast.9, bf16[1,2048,1024]{2,1,0:T(8,128)(2,1)} %w_gate.1, bf16[1,2048,1024]{2,1,0:T(8,128)(2,1)} %w_up.1, bf16[1,1024,2048]{2,1,0:T(8,128)(2,1)} %w_down.1, ...), custom_call_target="tpu_custom_call" | custom-call | tf_op jit(solution)/shard_map/pallas_call | solution.py:380
  104.6 1.9 %copy.12 = bf16[128,2048]{1,0:T(8,128)(2,1)} copy(bf16[128,2048]{1,0:T(8,128)(2,1)} %shard_map.100) | data formatting | bytes 1048576

commit v3 on v2

--- a/solution.py
+++ b/solution.py
@@ -37,9 +37,10 @@
     side, cores, cols,
     tokens, gain, ids, weight, w_gate, w_up, w_down, d_up, d_down, branch,
     out,
-    ag, mine, info, send, recv, result, back, rs_out, rs_in, high_t, low_t, dense, v_gate, v_up, v_down, wide,
+    ag, mine, info, send, recv, result, back, rs_out, rs_in, folded, shares, dense, v_gate, v_up, v_down, wide,
     ready, local_sem, info_send, info_recv, ag_send, ag_recv, out_send, out_recv, own_sem,
     ret_send, ret_recv, rs_send, rs_recv, w_send, w_recv,
+    pass_send, pass_recv, fold_send, fold_recv, on_send, on_recv,
 ):
     rows, width = tokens.shape
     plane = side * side * cores
@@ -141,8 +142,8 @@
         share = jnp.where(table0, facts[2:3, :], 0.0) + jnp.where(table1, facts[3:4, :], 0.0)
         share = share.T
         high = share.astype(BF16)
-        high_t[k, d] = high
-        low_t[k, d] = (share - high.astype(F32)).astype(BF16)
+        shares[k, d, :rows] = high
+        shares[k, d, rows:] = (share - high.astype(F32)).astype(BF16)
 
     def core_first(o):
         return (o[3], *o[:3])
@@ -153,12 +154,11 @@
     def slot_rows(group, j):
         return (0 if group == 0 else others, *j)
 
-    def dispatch(k, group, j):
+    def dispatch(k, group, d, j):
         return remote(
-            send6.at[(*slot_rows(group, j), slice(None), lanes[k])],
-            recv6.at[(*sources(k, group, j), slice(None), lanes[k])],
-            out_send.at[group + j[2] * (group > 0), k], out_recv.at[group + j[2] * (group > 0), k],
-            dev(with_dim(k, 0, *j)),
+            send6.at[(d, *j, slice(None), lanes[k])],
+            recv6.at[(*core_first(with_dim(k, d, *j)), slice(None), lanes[k])],
+            out_send.at[group, k], out_recv.at[group, k], dev(with_dim(k, 0, *j)),
         )
 
     here = (0, 0, 0)
@@ -170,11 +170,21 @@
             own_sem.at[group, k],
         )
 
-    def start_group(group, targets):
+    def turns(targets):
         count = len(targets)
-        for i in range(count):
-            for k in range(3):
-                dispatch(k, group, targets[(i + k * count // 3) % count]).start()
+        return [(k, targets[(i + k * count // 3) % count]) for i in range(count) for k in range(3)]
+
+    def start_own(e):
+        for k, j in turns(of_core[e]):
+            dispatch(k, 0, 0, j).start()
+
+    def start_ring(e):
+        def round_of(d, carry):
+            for k, j in turns(of_core[e]):
+                dispatch(k, 1 + e, d, j).start()
+            return carry
+
+        lax.fori_loop(1, side, round_of, 0)
 
     def bulk(buffer, k, blocks, s, r):
         part_of = buffer.at[pl.ds(0, blocks), :, lanes[k]]
@@ -199,7 +209,18 @@
     for d in ring:
         for k in range(3):
             tell(k, d).start()
-    for d in ring:
+    half = rows // 2
+    beside = (1, side - 1)
+
+    def pass_on(k, i):
+        d = beside[i]
+        part_of = pl.ds(i * half, half)
+        return remote(
+            ag.at[d, part_of, lanes[k]], ag.at[2, part_of, lanes[k]],
+            pass_send.at[k, i], pass_recv.at[k, i], dev(along(k, d)),
+        )
+
+    for d in beside:
         for k in range(3):
             share_tokens(k, d).start()
 
@@ -211,22 +232,32 @@
     )
 
     def piece_copy(p, stage, d, incoming):
-        half, lo, hi, turn = pieces[p]
+        which, lo, hi, turn = pieces[p]
         axis = turn[stage]
         where = list(at)
         for held in turn[:stage]:
             where[held] = slice(None)
         if incoming:
             where[axis] = (at[axis] + dims[axis] - d) % dims[axis]
-        block = wide.at[(half, *where, slice(None), pl.ds(lo, hi - lo))]
+        block = wide.at[(which, *where, slice(None), pl.ds(lo, hi - lo))]
         offset = along(axis, d)
         return remote(block, block, w_send.at[p, stage, d], w_recv.at[p, stage, d], dev(offset))
 
     def each(stage, act, incoming=False):
         for p in range(4):
             axis = pieces[p][3][stage]
-            for d in range(1, dims[axis]):
+            for d in beside if stage == 2 else range(1, dims[axis]):
                 act(piece_copy(p, stage, d, incoming))
+
+    def piece_on(p, i, incoming):
+        which, lo, hi, turn = pieces[p]
+        axis = turn[2]
+        where = list(at)
+        where[turn[0]] = pl.ds(i * (side // 2), side // 2)
+        where[turn[1]] = slice(None)
+        where[axis] = (at[axis] + side - (2 if incoming else beside[i])) % side
+        block = wide.at[(which, *where, slice(None), pl.ds(lo, hi - lo))]
+        return remote(block, block, on_send.at[p, i], on_recv.at[p, i], dev(along(axis, beside[i])))
 
     def begin(stage):
         each(stage, lambda copy: copy.start())
@@ -239,20 +270,27 @@
 
     begin(0)
     pl.semaphore_wait(ready, len(line))
-    start_group(0, order)
-    for k in range(3):
-        keep(k, 0).start()
-
-    for d in ring:
+    start_own(0)
+
+    for i in range(2):
+        for k in range(3):
+            share_tokens(k, beside[i]).wait_recv()
+            pass_on(k, i).start()
+    start_own(1)
+    for d in beside:
         for k in range(3):
             tell(k, d).wait_recv()
-            share_tokens(k, d).wait_recv()
             pack(k, d, info[k, d])
-        if d == ring[0]:
-            arrive(0)
-            begin(1)
+    arrive(0)
+    begin(1)
+    for k in range(3):
+        keep(k, 0).start()
+        tell(k, 2).wait_recv()
+        for i in range(2):
+            pass_on(k, i).wait_recv()
+        pack(k, 2, info[k, 2])
     for e in range(cores):
-        start_group(1, of_core[e])
+        start_ring(e)
     for k in range(3):
         keep(k, 1).start()
     arrive(1)
@@ -272,23 +310,34 @@
         res = jnp.dot(hidden, v_down[...], preferred_element_type=F32)
         result[block] = res.reshape(part_rows, CAP, width).astype(BF16)
 
-    def giveback(k, d, j):
-        group = 0 if isinstance(d, int) and d == 0 else 1
-        there = minus(with_dim(k, 0, *j))
-        src = result6.at[(*core_first(with_dim(k, d, *j)), slice(None), lanes[k])]
-        dst = back6.at[(d, *j, slice(None), lanes[k])]
-        if j == here:
-            return pltpu.make_async_copy(src, dst, own_sem.at[2, k] if group == 0 else own_sem.at[3, k])
-        return remote(src, dst, ret_send.at[group, k], ret_recv.at[group, k], dev(there))
+    def giveback(k, group, d, j):
+        return remote(
+            result6.at[(*core_first(with_dim(k, d, *j)), slice(None), lanes[k])],
+            back6.at[(d, *j, slice(None), lanes[k])],
+            ret_send.at[group, k], ret_recv.at[group, k], dev(minus(with_dim(k, 0, *j))),
+        )
+
+    def keep_back(k, group):
+        d = others if group else 0
+        return pltpu.make_async_copy(
+            result6.at[(*core_first(with_dim(k, d, *here)), slice(None), lanes[k])],
+            back6.at[(d, *here, slice(None), lanes[k])], own_sem.at[2 + group, k],
+        )
 
     def wait_group(group, k, blocks):
         bulk(recv, k, blocks, out_send.at[group, k], out_recv.at[group, k]).wait_recv()
 
-    def start_back(d, targets):
-        count = len(targets)
-        for i in range(count):
-            for k in range(3):
-                giveback(k, d, targets[(i + k * count // 3) % count]).start()
+    def back_own(e):
+        for k, j in turns(of_core[e]):
+            giveback(k, 0, 0, j).start()
+
+    def back_ring(e):
+        def round_of(d, carry):
+            for k, j in turns(of_core[e]):
+                giveback(k, 1, d, j).start()
+            return carry
+
+        lax.fori_loop(1, side, round_of, 0)
 
     for e in range(cores):
         for k in range(3):
@@ -299,20 +348,21 @@
             wait_group(1 + e, k, len(of_core[e]) * (side - 1))
         for p in range(2):
             experts_on(e * 2 + p)
-        start_back(others, of_core[e])
-    start_back(0, order)
-    for k in range(3):
-        giveback(k, others, here).start()
-        giveback(k, 0, here).start()
-
+        back_ring(e)
     arrive(2)
-    begin(3)
+    for p in range(4):
+        for i in range(2):
+            piece_on(p, i, False).start()
+    back_own(0)
+    for k in range(3):
+        keep_back(k, 1).start()
+        keep_back(k, 0).start()
 
     def combine(k, d):
         lo, hi = cols[k]
         rows_back = back[d * plane:(d + 1) * plane, :, lo:hi].reshape(slots, hi - lo)
-        total = jnp.dot(high_t[k, d], rows_back, preferred_element_type=F32)
-        return total + jnp.dot(low_t[k, d], rows_back, preferred_element_type=F32)
+        total = jnp.dot(shares[k, d], rows_back, preferred_element_type=F32)
+        return total[:rows] + total[rows:]
 
     def partial(k, d):
         return remote(
@@ -320,13 +370,35 @@
             dev(along(k, -d % side)),
         )
 
-    for k in range(3):
-        giveback(k, others, here).wait()
+    def fold(k, i):
+        part_of = pl.ds(i * half, half)
+        return remote(
+            rs_out.at[2, part_of, lanes[k]], folded.at[i, :, lanes[k]],
+            fold_send.at[k, i], fold_recv.at[k, i], dev(along(k, -beside[i] % side)),
+        )
+
+    for k in range(3):
+        lo, hi = cols[k]
+        keep_back(k, 1).wait()
         bulk(back, k, peers * (side - 1), ret_send.at[1, k], ret_recv.at[1, k]).wait_recv()
-        for d in ring:
-            lo, hi = cols[k]
-            rs_out[d, :, lo:hi] = combine(k, d).astype(BF16)
-            partial(k, d).start()
+        rs_out[2, :, lo:hi] = combine(k, 2).astype(BF16)
+        for i in range(2):
+            fold(k, i).start()
+    back_own(1)
+    for p in range(4):
+        for i in range(2):
+            piece_on(p, i, True).wait_recv()
+    begin(3)
+    for k in range(3):
+        lo, hi = cols[k]
+        for i in range(2):
+            total = combine(k, beside[i])
+            fold(k, i).wait_recv()
+            mixed = total[i * half:(i + 1) * half] + folded[i, :, lo:hi].astype(F32)
+            rest = total[(1 - i) * half:(2 - i) * half]
+            rs_out[beside[i], i * half:(i + 1) * half, lo:hi] = mixed.astype(BF16)
+            rs_out[beside[i], (1 - i) * half:(2 - i) * half, lo:hi] = rest.astype(BF16)
+            partial(k, beside[i]).start()
 
     arrive(3)
     dense_pre = jnp.dot(ag[0], wide[0].reshape(width, -1), preferred_element_type=F32)
@@ -337,10 +409,10 @@
     dense[...] = jnp.tanh(branch[...]) * dense_out
     for k in range(3):
         lo, hi = cols[k]
-        giveback(k, 0, here).wait()
+        keep_back(k, 0).wait()
         bulk(back, k, peers, ret_send.at[0, k], ret_recv.at[0, k]).wait_recv()
         total = combine(k, 0) + dense[:, lo:hi]
-        for d in ring:
+        for d in beside:
             partial(k, d).wait_recv()
             total = total + rs_in[d, :, lo:hi].astype(F32)
         out[:, lo:hi] = total.astype(BF16)
@@ -348,8 +420,11 @@
     for k in range(3):
         for d in ring:
             tell(k, d).wait_send()
-            share_tokens(k, d).wait_send()
-            partial(k, d).wait_send()
+        for i in range(2):
+            share_tokens(k, beside[i]).wait_send()
+            pass_on(k, i).wait_send()
+            fold(k, i).wait_send()
+            partial(k, beside[i]).wait_send()
         for e in range(cores):
             blocks = len(of_core[e]) * (side - 1)
             bulk(send, k, blocks, out_send.at[1 + e, k], out_recv.at[1 + e, k]).wait_send()
@@ -359,6 +434,9 @@
             bulk(result, k, blocks, ret_send.at[group, k], ret_recv.at[group, k]).wait_send()
     for stage in range(4):
         leave(stage)
+    for p in range(4):
+        for i in range(2):
+            piece_on(p, i, False).wait_send()
 
 
 def on_device(tokens, norm_gain, route_ids, route_weight, expert_gate, expert_up, expert_down, dense_up, dense_down, branch_gate):
@@ -369,7 +447,7 @@
     d_rows, dh = dense_up.shape
     cores = 2
     side = round((n // cores) ** (1 / 3))
-    assert side ** 3 * cores == n
+    assert side == 4 and side ** 3 * cores == n
     tile = width // 128
     cuts = [tile // 3, tile // 3 * 2, tile]
     cols = tuple((lo * 128, hi * 128) for lo, hi in zip([0, *cuts[:2]], cuts))
@@ -392,8 +470,8 @@
             pltpu.VMEM((n, CAP, width), BF16),
             pltpu.VMEM((side, rows, width), BF16),
             pltpu.VMEM((side, rows, width), BF16),
-            pltpu.VMEM((3, side, rows, plane * CAP), BF16),
-            pltpu.VMEM((3, side, rows, plane * CAP), BF16),
+            pltpu.VMEM((2, rows // 2, width), BF16),
+            pltpu.VMEM((3, side, 2 * rows, plane * CAP), BF16),
             pltpu.VMEM((rows, width), F32),
             pltpu.VMEM((width, ff), BF16),
             pltpu.VMEM((width, ff), BF16),
@@ -404,6 +482,7 @@
             dma((1 + cores, 3)), dma((1 + cores, 3)), dma((4, 3)),
             dma((2, 3)), dma((2, 3)), dma((3, side)), dma((3, side)),
             dma((4, 4, side)), dma((4, 4, side)),
+            dma((3, 2)), dma((3, 2)), dma((3, 2)), dma((3, 2)), dma((4, 2)), dma((4, 2)),
         ],
         compiler_params=pltpu.CompilerParams(
             collective_id=0, has_side_effects=True, vmem_limit_bytes=62 * 1024 * 1024

time: 107 us -> 97 us (0.907)
  the two profiles are of different devices: /device:TPU:8 before, /device:TPU:1 now
where the time goes in v3:
time: 97 us; the launch traced here: 96.8 us
  Pallas kernels  94.9 us (98%)
  local copies, waits for them, and re-layouts  1.88 us (2%)
    pallas_call x1, Pallas kernels, on_device(): pl.pallas_call(functools.partial(kernel, side, cores, cols), out_shape=ja...  94.9 us

profile of v3, /device:TPU:1, one launch (start us, length us, event | category | flops | bytes accessed | tf_op | source)
XLA Modules:
  0.0 96.8 jit_solution(4188109374871161216)
XLA Ops:
  0.0 94.9 %shard_map.100 = bf16[128,2048]{1,0:T(8,128)(2,1)} custom-call(bf16[128,2048]{1,0:T(8,128)(2,1)} %tokens.1, f32[1,2048]{1,0:T(1,128)} %bitcast.6, s32[2,128]{1,0:T(2,128)} %bitcast.8, f32[2,128]{1,0:T(2,128)} %bitcast.9, bf16[1,2048,1024]{2,1,0:T(8,128)(2,1)} %w_gate.1, bf16[1,2048,1024]{2,1,0:T(8,128)(2,1)} %w_up.1, bf16[1,1024,2048]{2,1,0:T(8,128)(2,1)} %w_down.1, ...), custom_call_target="tpu_custom_call" | custom-call | tf_op jit(solution)/shard_map/pallas_call | solution.py:458
  94.9 1.9 %copy.12 = bf16[128,2048]{1,0:T(8,128)(2,1)} copy(bf16[128,2048]{1,0:T(8,128)(2,1)} %shard_map.100) | data formatting | bytes 1048576

commit v4 on v3

--- a/solution.py
+++ b/solution.py
@@ -37,10 +37,10 @@
     side, cores, cols,
     tokens, gain, ids, weight, w_gate, w_up, w_down, d_up, d_down, branch,
     out,
-    ag, mine, info, send, recv, result, back, rs_out, rs_in, folded, shares, dense, v_gate, v_up, v_down, wide,
+    ag, mine, info, send, recv, result, back, rs_out, rs_in, folded, shares, dense, mixed_rows, v_gate, v_up, v_down, wide,
     ready, local_sem, info_send, info_recv, ag_send, ag_recv, out_send, out_recv, own_sem,
     ret_send, ret_recv, rs_send, rs_recv, w_send, w_recv,
-    pass_send, pass_recv, fold_send, fold_recv, on_send, on_recv,
+    pass_send, pass_recv, fold_send, fold_recv, on_send, on_recv, emit_sem,
 ):
     rows, width = tokens.shape
     plane = side * side * cores
@@ -225,8 +225,8 @@
             share_tokens(k, d).start()
 
     pieces = (
-        (0, 0, 384, (0, 1, 2, 3)),
-        (0, 384, 512, (1, 2, 0, 3)),
+        (0, 0, 256, (0, 1, 2, 3)),
+        (0, 256, 512, (1, 0, 2, 3)),
         (1, 0, 256, (1, 2, 0, 3)),
         (1, 256, 512, (2, 0, 1, 3)),
     )
@@ -411,11 +411,19 @@
         lo, hi = cols[k]
         keep_back(k, 0).wait()
         bulk(back, k, peers, ret_send.at[0, k], ret_recv.at[0, k]).wait_recv()
-        total = combine(k, 0) + dense[:, lo:hi]
+        dense[:, lo:hi] += combine(k, 0)
+
+    def emit(k):
+        return pltpu.make_async_copy(mixed_rows.at[:, lanes[k]], out.at[:, lanes[k]], emit_sem.at[k])
+
+    for k in range(3):
+        lo, hi = cols[k]
+        total = dense[:, lo:hi]
         for d in beside:
             partial(k, d).wait_recv()
             total = total + rs_in[d, :, lo:hi].astype(F32)
-        out[:, lo:hi] = total.astype(BF16)
+        mixed_rows[:, lo:hi] = total.astype(BF16)
+        emit(k).start()
 
     for k in range(3):
         for d in ring:
@@ -437,6 +445,8 @@
     for p in range(4):
         for i in range(2):
             piece_on(p, i, False).wait_send()
+    for k in range(3):
+        emit(k).wait()
 
 
 def on_device(tokens, norm_gain, route_ids, route_weight, expert_gate, expert_up, expert_down, dense_up, dense_down, branch_gate):
@@ -459,7 +469,7 @@
         functools.partial(kernel, side, cores, cols),
         out_shape=jax.ShapeDtypeStruct((rows, width), BF16),
         in_specs=[vmem, vmem, vmem, vmem, hbm, hbm, hbm, hbm, hbm, vmem],
-        out_specs=vmem,
+        out_specs=hbm,
         scratch_shapes=[
             pltpu.VMEM((side, rows, width), BF16),
             pltpu.VMEM((8, rows), F32),
@@ -473,6 +483,7 @@
             pltpu.VMEM((2, rows // 2, width), BF16),
             pltpu.VMEM((3, side, 2 * rows, plane * CAP), BF16),
             pltpu.VMEM((rows, width), F32),
+            pltpu.VMEM((rows, width), BF16),
             pltpu.VMEM((width, ff), BF16),
             pltpu.VMEM((width, ff), BF16),
             pltpu.VMEM((ff, width), BF16),
@@ -482,7 +493,7 @@
             dma((1 + cores, 3)), dma((1 + cores, 3)), dma((4, 3)),
             dma((2, 3)), dma((2, 3)), dma((3, side)), dma((3, side)),
             dma((4, 4, side)), dma((4, 4, side)),
-            dma((3, 2)), dma((3, 2)), dma((3, 2)), dma((3, 2)), dma((4, 2)), dma((4, 2)),
+            dma((3, 2)), dma((3, 2)), dma((3, 2)), dma((3, 2)), dma((4, 2)), dma((4, 2)), dma((3,)),
         ],
         compiler_params=pltpu.CompilerParams(
             collective_id=0, has_side_effects=True, vmem_limit_bytes=62 * 1024 * 1024

time: 97 us -> 95.8 us (0.988)
  Pallas kernels: 94.9 us -> 93.8 us
    pallas_call x1, Pallas kernels: 94.9 us -> 93.8 us  [on_device(): pl.pallas_call(functools.partial(kernel, side, cores, cols), out_shape=ja...]
where the time goes in v4:
time: 95.8 us; the launch traced here: 95.7 us
  Pallas kernels  93.8 us (98%)
  local copies, waits for them, and re-layouts  1.88 us (2%)
    pallas_call x1, Pallas kernels, on_device(): pl.pallas_call(functools.partial(kernel, side, cores, cols), out_shape=ja...  93.8 us

profile of v4, /device:TPU:1, one launch (start us, length us, event | category | flops | bytes accessed | tf_op | source)
XLA Modules:
  0.0 95.7 jit_solution(45313366096757290)
XLA Ops:
  0.0 93.8 %shard_map.100 = bf16[128,2048]{1,0:T(8,128)(2,1)} custom-call(bf16[128,2048]{1,0:T(8,128)(2,1)} %tokens.1, f32[1,2048]{1,0:T(1,128)} %bitcast.6, s32[2,128]{1,0:T(2,128)} %bitcast.8, f32[2,128]{1,0:T(2,128)} %bitcast.9, bf16[1,2048,1024]{2,1,0:T(8,128)(2,1)} %w_gate.1, bf16[1,2048,1024]{2,1,0:T(8,128)(2,1)} %w_up.1, bf16[1,1024,2048]{2,1,0:T(8,128)(2,1)} %w_down.1, ...), custom_call_target="tpu_custom_call" | custom-call | tf_op jit(solution)/shard_map/pallas_call | solution.py:468
  93.8 1.9 %copy.12 = bf16[128,2048]{1,0:T(8,128)(2,1)} copy(bf16[128,2048]{1,0:T(8,128)(2,1)} %shard_map.100) | data formatting | bytes 1048576

commit v5 on v4

--- a/solution.py
+++ b/solution.py
@@ -289,12 +289,12 @@
         for i in range(2):
             pass_on(k, i).wait_recv()
         pack(k, 2, info[k, 2])
-    for e in range(cores):
-        start_ring(e)
-    for k in range(3):
-        keep(k, 1).start()
+    start_ring(0)
     arrive(1)
     begin(2)
+    start_ring(1)
+    for k in range(3):
+        keep(k, 1).start()
 
     for load in loads:
         load.wait()

time: 95.8 us -> 95.6 us (level)
  no operation moved by 1% of the time
where the time goes in v5:
time: 95.6 us; the launch traced here: 95.4 us
  Pallas kernels  93.5 us (98%)
  local copies, waits for them, and re-layouts  1.88 us (2%)
    pallas_call x1, Pallas kernels, on_device(): pl.pallas_call(functools.partial(kernel, side, cores, cols), out_shape=ja...  93.5 us

profile of v5, /device:TPU:1, one launch (start us, length us, event | category | flops | bytes accessed | tf_op | source)
XLA Modules:
  0.0 95.4 jit_solution(17149376374405406986)
XLA Ops:
  0.0 93.5 %shard_map.100 = bf16[128,2048]{1,0:T(8,128)(2,1)} custom-call(bf16[128,2048]{1,0:T(8,128)(2,1)} %tokens.1, f32[1,2048]{1,0:T(1,128)} %bitcast.6, s32[2,128]{1,0:T(2,128)} %bitcast.8, f32[2,128]{1,0:T(2,128)} %bitcast.9, bf16[1,2048,1024]{2,1,0:T(8,128)(2,1)} %w_gate.1, bf16[1,2048,1024]{2,1,0:T(8,128)(2,1)} %w_up.1, bf16[1,1024,2048]{2,1,0:T(8,128)(2,1)} %w_down.1, ...), custom_call_target="tpu_custom_call" | custom-call | tf_op jit(solution)/shard_map/pallas_call | solution.py:468
  93.5 1.9 %copy.12 = bf16[128,2048]{1,0:T(8,128)(2,1)} copy(bf16[128,2048]{1,0:T(8,128)(2,1)} %shard_map.100) | data formatting | bytes 1048576
